TPU v7x, 32 devices: a whole 2x2x4 slice. The times are simulated.
32 devices in a mesh: grp: 2 (over y), ep: 4 (over z), tp: 4 (over x, core).
Axes of the slice: x: 2, y: 2, z: 4, core: 2. Of those that a mesh axis runs over, the one named last changes fastest.
Arguments:
- query_rows: bfloat16 [1536, 2048], P(('grp', 'ep'), 'tp'), parts along dimension 0, may hold values from -100 to 100
- projected_keys: bfloat16 [1536, 512], P(('grp', 'ep'), 'tp'), parts along dimension 0, may hold values from -100 to 100
- projected_values: bfloat16 [1536, 512], P(('grp', 'ep'), 'tp'), parts along dimension 0, may hold values from -6 to 6
- query_gain: float32 [128], replicated, may hold values from 0.3 to 6.5
- key_norm_gain: float32 [128], replicated, may hold values from 0.3 to 6.5
- out_proj: bfloat16 [2048, 2048], P('tp'), may hold values from -4 to 4
- mix_tokens: bfloat16 [4096, 2048], P(('grp', 'ep', 'tp')), parts along dimension 0, may hold values from -150 to 150
- norm_gain: float32 [2048], replicated, may hold values from 0.1 to 1.9
- expert_ids: int32 [4096, 2], P(('grp', 'ep', 'tp')), parts along dimension 0, may hold values from 0 to 3, all different within a row; in each aligned block of 128 rows (0 to 127, 128 to 255, ...) at most 96 rows name the same one
- expert_score: float32 [4096, 2], P(('grp', 'ep', 'tp')), parts along dimension 0, may hold values from -6 to 6
- gate_proj: bfloat16 [4, 2048, 2048], P('ep', None, 'tp'), may hold values from -0.125 to 0.125
- up_proj: bfloat16 [4, 2048, 2048], P('ep', None, 'tp'), may hold values from -0.125 to 0.125
- down_proj: bfloat16 [4, 2048, 2048], P('ep', 'tp'), may hold values from -0.125 to 0.125
Outputs:
- mixed_rows: bfloat16 [1536, 2048], P(('grp', 'ep', 'tp')), parts along dimension 0
- expert_out: bfloat16 [4096, 2048], P(('grp', 'ep', 'tp')), parts along dimension 0
There are 2 independent parts, one for each index of `grp`. A program takes and returns all parts, laid end to end along the dimension named above; an argument that names none is the same for every part. Nothing has to cross between parts.
Inputs may be any that keep to these rules, and one draw needn't show every extreme that they name: `expert_ids`: each row names 2 different experts. Within the rows of one device (aligned blocks of 128 rows) no expert is named more than 96 times, and in every draw some device names some expert exactly 96 times.
All inputs are finite; a program needn't handle non-finite values.
Results may differ from a plain program's by a relative error of at most 0.014.
The roundings to bfloat16 on the way count: a program that leaves them out, or rounds other values in their place, can miss the bound.
Values may be sent and summed in bfloat16 or wider, within the bound.
A program may use at most 128 MiB of HBM per device.

v0:
```python
import math
import jax
import jax.numpy as jnp
from jax import lax
from jax.sharding import PartitionSpec as P

GRID_W = 64
EPS = 1e-06
THETA = 10000.0


def head_norm(vectors, gain):
    return vectors * lax.rsqrt(jnp.mean(vectors * vectors, axis=-1, keepdims=True) + EPS) * gain


def rotate_grid(vectors, token_positions):
    length, heads, head_dim = vectors.shape
    quarter = head_dim // 4
    freqs = 1.0 / THETA ** (jnp.arange(quarter, dtype=jnp.float32) * 4.0 / head_dim)
    grid_row = (token_positions // GRID_W).astype(jnp.float32)
    grid_col = (token_positions % GRID_W).astype(jnp.float32)
    angles = jnp.stack([grid_row[:, None] * freqs, grid_col[:, None] * freqs], axis=1)
    cosine = jnp.cos(angles)[:, None]
    sine = jnp.sin(angles)[:, None]
    halves = vectors.reshape(length, heads, 2, 2, quarter)
    first = halves[..., 0, :]
    second = halves[..., 1, :]
    turned = jnp.stack([first * cosine - second * sine, second * cosine + first * sine], axis=-2)
    return turned.reshape(length, heads, head_dim)


def prepare_inputs(raw_rows, gain, heads, token_positions):
    length = raw_rows.shape[0]
    head_dim = gain.shape[0]
    vectors = raw_rows.astype(jnp.float32).reshape(length, heads, head_dim)
    return rotate_grid(head_norm(vectors, gain), token_positions).astype(jnp.bfloat16)


def mixer_half(query_rows, projected_keys, projected_values, query_gain, key_norm_gain, out_proj):
    length = query_rows.shape[0]
    head_dim = query_gain.shape[0]
    kv_heads = projected_keys.shape[1] // head_dim
    q_heads = query_rows.shape[1] // head_dim
    queries_per_group = q_heads // kv_heads
    token_positions = lax.axis_index("ep") * length + jnp.arange(length, dtype=jnp.int32)
    query_matrix = prepare_inputs(query_rows, query_gain, q_heads, token_positions).reshape(
        length, kv_heads, queries_per_group, head_dim
    )
    keys_turned = prepare_inputs(projected_keys, key_norm_gain, kv_heads, token_positions).reshape(
        length, kv_heads * head_dim
    )
    score_scale = head_dim ** (-0.5)
    initial = (
        jnp.full((kv_heads, queries_per_group, length), -1e30, jnp.float32),
        jnp.zeros((kv_heads, queries_per_group, length), jnp.float32),
        jnp.zeros((length, kv_heads, queries_per_group, head_dim), jnp.float32),
    )
    width = kv_heads * head_dim
    pair = lax.all_gather(
        jnp.concatenate([keys_turned, projected_values], axis=1), "ep", axis=0, tiled=True
    )
    key_piece = pair[:, :width]
    value_piece = pair[:, width:]
    piece_rows = key_piece.shape[0]
    step_rows = math.gcd(piece_rows, 1024)

    def one_block(block_index, running):
        run_max, run_sum, run_acc = running
        offset = block_index * step_rows
        key_block = lax.dynamic_slice_in_dim(key_piece, offset, step_rows, 0).reshape(
            step_rows, kv_heads, head_dim
        )
        value_block = lax.dynamic_slice_in_dim(value_piece, offset, step_rows, 0).reshape(
            step_rows, kv_heads, head_dim
        )
        scores = (
            jnp.einsum(
                "tkgd,skd->kgts", query_matrix, key_block, preferred_element_type=jnp.float32
            )
            * score_scale
        )
        new_max = jnp.maximum(run_max, jnp.max(scores, axis=-1))
        factor = jnp.exp(run_max - new_max)
        weights = jnp.exp(scores - new_max[..., None])
        run_sum = run_sum * factor + jnp.sum(weights, axis=-1)
        update = jnp.einsum(
            "kgts,skd->tkgd",
            weights.astype(jnp.bfloat16),
            value_block,
            preferred_element_type=jnp.float32,
        )
        run_acc = run_acc * jnp.transpose(factor, (2, 0, 1))[..., None] + update
        return (new_max, run_sum, run_acc)

    run_max, run_sum, run_acc = lax.fori_loop(0, piece_rows // step_rows, one_block, initial)
    heads_out = (
        (run_acc / jnp.transpose(run_sum, (2, 0, 1))[..., None])
        .astype(jnp.bfloat16)
        .reshape(length, q_heads * head_dim)
    )
    return jnp.dot(heads_out, out_proj, preferred_element_type=jnp.float32).astype(jnp.bfloat16)


def both_halves(
    query_rows,
    projected_keys,
    projected_values,
    query_gain,
    key_norm_gain,
    out_proj,
    mix_tokens,
    norm_gain,
    expert_ids,
    expert_score,
    gate_proj,
    up_proj,
    down_proj,
):
    length, model_dim = mix_tokens.shape
    top_count = expert_ids.shape[1]
    local_experts = gate_proj.shape[0]
    expert_axis = lax.axis_size("ep")
    experts_all = expert_axis * local_experts
    capacity = length * top_count * 3 // (2 * experts_all)
    values_b = mix_tokens.astype(jnp.float32)
    normed = (
        values_b
        * lax.rsqrt(jnp.mean(values_b * values_b, axis=-1, keepdims=True) + EPS)
        * norm_gain
    ).astype(jnp.bfloat16)
    flat = expert_ids.reshape(length * top_count)
    onehot = (flat[:, None] == jnp.arange(experts_all, dtype=jnp.int32)).astype(jnp.int32)
    slots = jnp.sum((jnp.cumsum(onehot, axis=0) - onehot) * onehot, axis=1)
    target = flat * capacity + slots
    placed = (target[:, None] == jnp.arange(experts_all * capacity, dtype=jnp.int32)).astype(
        jnp.int32
    )
    placed = jnp.sum(placed.reshape(length, top_count, experts_all * capacity), axis=1).astype(
        jnp.bfloat16
    )
    outgoing = jnp.einsum("re,rd->ed", placed, normed, preferred_element_type=jnp.float32).astype(
        jnp.bfloat16
    )
    outgoing = outgoing.reshape(expert_axis, local_experts, capacity, model_dim)
    arrived = lax.all_to_all(outgoing, "ep", split_axis=0, concat_axis=0, tiled=True)
    arrived, query_rows, projected_keys, projected_values = lax.optimization_barrier(
        (arrived, query_rows, projected_keys, projected_values)
    )
    rows_in = lax.all_gather(arrived, "tp", axis=0, tiled=True)
    head_partial = mixer_half(
        query_rows, projected_keys, projected_values, query_gain, key_norm_gain, out_proj
    )
    rows_in, head_partial = lax.optimization_barrier((rows_in, head_partial))
    mixed_rows = lax.psum_scatter(head_partial, "tp", scatter_dimension=0, tiled=True)
    gate_out = jnp.einsum("secd,edf->secf", rows_in, gate_proj, preferred_element_type=jnp.float32)
    up_out = jnp.einsum("secd,edf->secf", rows_in, up_proj, preferred_element_type=jnp.float32)
    active = (jax.nn.silu(gate_out) * up_out).astype(jnp.bfloat16)
    summed = lax.psum_scatter(
        jnp.einsum("secf,efd->secd", active, down_proj, preferred_element_type=jnp.float32).astype(
            jnp.bfloat16
        ),
        "tp",
        scatter_dimension=0,
        tiled=True,
    )
    returned = lax.all_to_all(summed, "ep", split_axis=0, concat_axis=0, tiled=True)
    results = returned.reshape(experts_all * capacity, model_dim)
    first_weight = jax.nn.sigmoid(expert_score[:, 0] - expert_score[:, 1])
    picks = target.reshape(length, top_count)
    chosen = [
        jnp.dot(
            (picks[:, k : k + 1] == jnp.arange(experts_all * capacity, dtype=jnp.int32)).astype(
                jnp.bfloat16
            ),
            results,
            preferred_element_type=jnp.float32,
        )
        for k in range(2)
    ]
    combined = first_weight[:, None] * chosen[0] + (1.0 - first_weight)[:, None] * chosen[1]
    return (mixed_rows, combined.astype(jnp.bfloat16))


def local(
    query_rows,
    projected_keys,
    projected_values,
    query_gain,
    key_norm_gain,
    out_proj,
    mix_tokens,
    norm_gain,
    expert_ids,
    expert_score,
    gate_proj,
    up_proj,
    down_proj,
):
    return both_halves(
        query_rows,
        projected_keys,
        projected_values,
        query_gain,
        key_norm_gain,
        out_proj,
        mix_tokens,
        norm_gain,
        expert_ids,
        expert_score,
        gate_proj,
        up_proj,
        down_proj,
    )


def solution(mesh):
    in_specs = (
        P(("grp", "ep"), "tp"),
        P(("grp", "ep"), "tp"),
        P(("grp", "ep"), "tp"),
        P(),
        P(),
        P("tp", None),
        P(("grp", "ep", "tp"), None),
        P(),
        P(("grp", "ep", "tp"), None),
        P(("grp", "ep", "tp"), None),
        P("ep", None, "tp"),
        P("ep", None, "tp"),
        P("ep", "tp", None),
    )
    out_specs = (P(("grp", "ep", "tp"), None), P(("grp", "ep", "tp"), None))
    return jax.shard_map(local, mesh=mesh, in_specs=in_specs, out_specs=out_specs, check_vma=False)
```

profile of v0, /device:TPU:0, one launch (start us, length us, event | category | flops | bytes accessed | tf_op | source)
XLA Modules:
  0.0 235.2 jit_solution(7432642397368163617)
XLA Ops:
  7.2 0.9 copy.77
  8.4 1.2 fusion.41
  9.7 1.2 reduce-window.6
  12.3 1.7 convolution_convert_fusion
  14.1 43.3 %all_to_all.10 = bf16[4,1,96,2048]{3,2,1,0:T(8,128)(2,1)} all-to-all(bf16[4,1,96,2048]{3,2,1,0:T(8,128)(2,1)S(1)} %bitcast.177), channel_id=1, replica_groups=mesh['grp'=2,'ep'=4,'tp'=4] {'ep'}, dimensions={0} | all-to-all | bytes 3145728 | tf_op jit(solution)/shard_map/all_to_all | solution.py:145
  59.5 15.1 %all_gather.7 = bf16[768,256]{1,0:T(8,128)(2,1)S(1)} all-gather(bf16[192,256]{1,0:T(8,128)(2,1)S(1)} %copy.85), channel_id=1, replica_groups=mesh['grp'=2,'ep'=4,'tp'=4] {'ep'}, dimensions={0}, use_global_device_ids=true | all-gather | bytes 491520 | tf_op jit(solution)/shard_map/all_gather | solution.py:59
  74.6 0.8 fusion.68
  75.3 8.8 %while.18 = (s32[]{:T(128)}, f32[1,4,192]{2,1,0:T(4,128)S(1)}, f32[1,4,192]{2,1,0:T(4,128)S(1)}, f32[192,1,4,128]{3,0,2,1:T(8,128)S(1)}, bf16[768,128]{1,0:T(8,1...) while((s32[]{:T(128)}, f32[1,4,192]{2,1,0:T(4,128)S(1)}, ...), condition=%wide.region_10.11_spmd.clone, body=%wide.region_7.10_spmd.clone.sunk | while | flops 102142472 | bytes 3522743 | solution.py:95
  75.3 1.2 fusion.80
  77.0 1.2 fusion.83
  78.3 1.2 fusion.80
  79.9 1.2 fusion.83
  81.2 1.3 fusion.80
  82.9 1.2 fusion.83
  84.4 3.1 %convolution_convert_fusion.1 = bf16[192,2048]{1,0:T(8,128)(2,1)} fusion(bf16[512,2048]{1,0:T(8,128)(2,1)} %param.20, bf16[24,8,4,128]{3,2,1,0:T(4,128)(2,1)S(1)} %bitcast.183), kind=kOutput, calls=%fused_computation.35 | convolution fusion | flops 403046400 | bytes 3080192 | tf_op jit(solution)/shard_map/dot_general | solution.py:101
  87.5 15.6 %all-gather.2.cloned.1.call-done = bf16[16,1,96,2048]{3,2,1,0:T(8,128)(2,1)} async-done(((bf16[4,1,96,2048]{3,2,1,0:T(8,128)(2,1)}), bf16[16,1,96,2048]{3,2,1,0:T(8,128)(2,1)}) %all-gather.2.cloned.1.call-update) | async-done | bytes 6291472 | tf_op jit(solution)/shard_map/all_gather | solution.py:149
  103.1 8.5 %fusion.15 = f32[16,96,512]{2,1,0:T(8,128)} fusion(bf16[16,1,96,2048]{3,2,1,0:T(8,128)(2,1)} %all-gather.2.cloned.1.call-done, bf16[1,2048,512]{2,1,0:T(8,128)(2,1)} %param.26), kind=kOutput, calls=%fused_computation.22 | convolution fusion | flops 3221225472 | bytes 11534336 | tf_op jit(solution)/shard_map/secd,edf->secf/dot_general | solution.py:156
  111.7 11.9 %convert_bitcast_fusion = bf16[16,1,96,2048]{3,2,0,1:T(8,128)(2,1)} fusion(bf16[1,512,2048]{2,1,0:T(8,128)(2,1)S(1)} %copy-done, f32[16,96,512]{2,1,0:T(8,128)} %fusion.15, bf16[1,2048,512]{2,1,0:T(8,128)(2,1)} %param.25, bf16[16,1,96,2048]{3,2,1,0:T(8,128)(2,1)} %all-gather.2.cloned.1.call-done), kind=kOutput, calls=%fused_computation.26 | convolution fusion | flops 6450315264 | bytes 19922944 | tf_op jit(solution)/shard_map/secf,efd->secd/dot_general | solution.py:159
  123.6 59.0 %reduce-scatter.5.cloned.1.call-done = bf16[4,1,96,2048]{3,2,0,1:T(8,128)(2,1)} async-done(((bf16[16,1,96,2048]{3,2,0,1:T(8,128)(2,1)}), bf16[4,1,96,2048]{3,2,0,1:T(8,128)(2,1)}) %reduce-scatter.5.cloned.1.call-update) | async-done | bytes 1572880 | tf_op jit(solution)/shard_map/reduce_scatter | solution.py:158
  182.6 4.6 %all-to-all-start.1 = ((bf16[4,1,96,2048]{3,2,1,0:T(8,128)(2,1)}), bf16[4,1,96,2048]{3,2,1,0:T(8,128)(2,1)}, u32[]{:S(2)}, u32[]{:S(2)}) async-start(bf16[4,1,96,2048]{3,2,1,0:T(8,128)(2,1)} %bitcast.181), calls=%async_computation.3 | async-start | bytes 3145728 | tf_op jit(solution)/shard_map/all_to_all | solution.py:166
  187.2 0.7 reduce-scatter.3.cloned.1.call-update
  187.9 36.1 %all-to-all-done.1 = bf16[4,1,96,2048]{3,2,1,0:T(8,128)(2,1)} async-done(((bf16[4,1,96,2048]{3,2,1,0:T(8,128)(2,1)}), bf16[4,1,96,2048]{3,2,1,0:T(8,128)(2,1)}, u32[]{:S(2)}, u32[]{:S(2)}) %all-to-all-start.1) | async-done | bytes 1572896 | tf_op jit(solution)/shard_map/all_to_all | solution.py:166
  224.1 1.9 convolution_multiply_fusion.2
  226.0 2.7 %fusion.24 = bf16[128,2048]{1,0:T(8,128)(2,1)} fusion(f32[128,2048]{1,0:T(8,128)S(1)} %convolution_multiply_fusion.2, bf16[384,2048]{1,0:T(8,128)(2,1)} %bitcast.35, f32[128]{0:T(128)S(1)} %get-tuple-element.216, s32[128]{0:T(128)S(1)} %get-tuple-element.232), kind=kOutput, calls=%fused_computation.39 | convolution fusion | flops 202162176 | bytes 3146752 | tf_op jit(solution)/shard_map/dot_general | solution.py:171
  (75 shorter events, 5.2 us)
Async XLA Ops:
  7.2 104.5 %copy-start = (bf16[1,512,2048]{2,1,0:T(8,128)(2,1)S(1)}, bf16[1,512,2048]{2,1,0:T(8,128)(2,1)}, u32[]{:S(2)}) copy-start(bf16[1,512,2048]{2,1,0:T(8,128)(2,1)} %param.27) | copy-start | bytes 6291460
  7.2 96.0 %all-gather.2.cloned.1.call-start = ((), (), s32[]{:S(2)}) async-start(), calls=%async_computation.4 | async-start | bytes 7864320 | tf_op jit(solution)/shard_map/all_gather | solution.py:149
  14.1 43.5 %copy-start.6 = (f32[128]{0:T(128)S(1)}, f32[128]{0:T(128)}, u32[]{:S(2)}) copy-start(f32[128]{0:T(128)} %param.18) | copy-start | bytes 1540
  14.1 43.9 %copy-start.2 = (bf16[192,128]{1,0:T(8,128)(2,1)S(1)}, bf16[192,128]{1,0:T(8,128)(2,1)}, u32[]{:S(2)}) copy-start(bf16[192,128]{1,0:T(8,128)(2,1)} %param.17) | copy-start | bytes 147460
  14.1 44.1 %copy-start.3 = (bf16[192,128]{1,0:T(8,128)(2,1)S(1)}, bf16[192,128]{1,0:T(8,128)(2,1)}, u32[]{:S(2)}) copy-start(bf16[192,128]{1,0:T(8,128)(2,1)} %param.16) | copy-start | bytes 147460
  14.1 44.2 %copy-start.5 = (f32[128]{0:T(128)S(1)}, f32[128]{0:T(128)}, u32[]{:S(2)}) copy-start(f32[128]{0:T(128)} %param.19) | copy-start | bytes 1540
  57.5 1.4 copy-start.1
  57.5 125.1 %reduce-scatter.5.cloned.1.call-start = ((), (), s32[]{:S(2)}) async-start(), calls=%async_computation.6 | async-start | bytes 7864320 | tf_op jit(solution)/shard_map/reduce_scatter | solution.py:158
  123.6 64.3 %copy-start.4 = (f32[128,2]{0,1:T(2,128)S(1)}, f32[128,2]{0,1:T(2,128)}, u32[]{:S(2)}) copy-start(f32[128,2]{0,1:T(2,128)} %param.24) | copy-start | bytes 3076
  182.6 41.5 %all-to-all-start.1 = ((bf16[4,1,96,2048]{3,2,1,0:T(8,128)(2,1)}), bf16[4,1,96,2048]{3,2,1,0:T(8,128)(2,1)}, u32[]{:S(2)}, u32[]{:S(2)}) async-start(bf16[4,1,96,2048]{3,2,1,0:T(8,128)(2,1)} %bitcast.181), calls=%async_computation.3 | async-start | bytes 3145728 | tf_op jit(solution)/shard_map/all_to_all | solution.py:166
  187.2 41.5 %reduce-scatter.3.cloned.1.call-start = ((), (), s32[]{:S(2)}) async-start(), calls=%async_computation.5 | async-start | bytes 983040 | tf_op jit(solution)/shard_map/reduce_scatter | solution.py:154
Sparse Core Ops, SparseCore 0:
  57.6 45.4 all-gather.1
  123.7 58.8 reduce-scatter.4
  191.1 23.7 reduce-scatter.2
where the time goes:
time: 236 us; the launch traced here: 235 us
  waiting for transfers between devices  111 us (47%)
  blocking collectives  58.4 us (25%)
  matrix products  37.2 us (16%)
  between operations  14 us (6%)
  other arithmetic  5.9 us (2%)
  starting transfers between devices  4.68 us (2%)
  local copies, waits for them, and re-layouts  3.36 us (1%)
    reduce_scatter x1, waiting for transfers between devices, both_halves(): lax.psum_scatter(jnp.einsum('secf,efd->secd', active, down_proj, preferre...  59 us
    all_to_all x1, blocking collectives, both_halves(): lax.all_to_all(outgoing, 'ep', split_axis=0, concat_axis=0, tiled=True)  43.3 us
    all_to_all x1, waiting for transfers between devices, both_halves(): lax.all_to_all(summed, 'ep', split_axis=0, concat_axis=0, tiled=True)  36.1 us
    all_gather x1, waiting for transfers between devices, both_halves(): rows_in = lax.all_gather(arrived, 'tp', axis=0, tiled=True)  15.6 us
    all_gather x1, blocking collectives, mixer_half(): lax.all_gather(jnp.concatenate([keys_turned, projected_values], axis=1),...  15.1 us
    dot_general x1, matrix products, both_halves(): jnp.einsum('secf,efd->secd', active, down_proj, preferred_element_type=jn...  11.9 us
    dot_general x1, matrix products, both_halves(): jnp.einsum('secd,edf->secf', rows_in, up_proj, preferred_element_type=jnp...  8.52 us
  transfers between devices with their start and end apart: 4, of which 3 were waited for; matrix products, arithmetic and copies ran while one was open for 8% of the time, Pallas kernels for 0%

commit v1 on v0

--- a/solution.py
+++ b/solution.py
@@ -56,8 +56,16 @@
         jnp.zeros((length, kv_heads, queries_per_group, head_dim), jnp.float32),
     )
     width = kv_heads * head_dim
-    pair = lax.all_gather(
-        jnp.concatenate([keys_turned, projected_values], axis=1), "ep", axis=0, tiled=True
+    pair = jnp.concatenate(
+        lax.all_to_all(
+            jnp.stack(
+                [jnp.concatenate([keys_turned, projected_values], axis=1)] * lax.axis_size("ep")
+            ),
+            "ep",
+            0,
+            0,
+        ),
+        axis=0,
     )
     key_piece = pair[:, :width]
     value_piece = pair[:, width:]

time: 236 us -> 236 us (level)
  blocking collectives: 58.4 us -> 43.3 us
  waiting for transfers between devices: 111 us -> 121 us
  starting transfers between devices: 4.68 us -> 8.15 us
    all_gather x1 -> x0, blocking collectives: 15.1 us -> none  [mixer_half(): lax.all_gather(jnp.concatenate([keys_turned, projected_values], axis=1),...]
    all_to_all x0 -> x1, waiting for transfers between devices: none -> 9.19 us  [mixer_half(): lax.all_to_all(jnp.stack([jnp.concatenate([keys_turned, projected_values]...]
    all_to_all x0 -> x1, starting transfers between devices: none -> 3.46 us  [mixer_half(): lax.all_to_all(jnp.stack([jnp.concatenate([keys_turned, projected_values]...]
  transfers between devices with their start and end apart: 4 -> 5, of which waited for: 3 -> 4; matrix products, arithmetic and copies ran while one was open for 8% -> 9% of each run, Pallas kernels for 0% -> 0%
where the time goes in v1:
time: 236 us; the launch traced here: 235 us
  waiting for transfers between devices  121 us (51%)
  blocking collectives  43.3 us (18%)
  matrix products  37.2 us (16%)
  between operations  14.1 us (6%)
  starting transfers between devices  8.15 us (3%)
  other arithmetic  5.9 us (2%)
  local copies, waits for them, and re-layouts  5.07 us (2%)
    reduce_scatter x1, waiting for transfers between devices, both_halves(): lax.psum_scatter(jnp.einsum('secf,efd->secd', active, down_proj, preferre...  59 us
    all_to_all x1, blocking collectives, both_halves(): lax.all_to_all(outgoing, 'ep', split_axis=0, concat_axis=0, tiled=True)  43.3 us
    all_to_all x1, waiting for transfers between devices, both_halves(): lax.all_to_all(summed, 'ep', split_axis=0, concat_axis=0, tiled=True)  36.1 us
    all_gather x1, waiting for transfers between devices, both_halves(): rows_in = lax.all_gather(arrived, 'tp', axis=0, tiled=True)  16.3 us
    dot_general x1, matrix products, both_halves(): jnp.einsum('secf,efd->secd', active, down_proj, preferred_element_type=jn...  11.9 us
    all_to_all x1, waiting for transfers between devices, mixer_half(): lax.all_to_all(jnp.stack([jnp.concatenate([keys_turned, projected_values]...  9.19 us
    dot_general x1, matrix products, both_halves(): jnp.einsum('secd,edf->secf', rows_in, up_proj, preferred_element_type=jnp...  8.52 us
  transfers between devices with their start and end apart: 5, of which 4 were waited for; matrix products, arithmetic and copies ran while one was open for 9% of the time, Pallas kernels for 0%

profile of v1, /device:TPU:0, one launch (start us, length us, event | category | flops | bytes accessed | tf_op | source)
XLA Modules:
  0.0 235.2 jit_solution(12678971696200661960)
XLA Ops:
  7.2 0.9 copy.75
  8.4 1.2 fusion.41
  9.7 1.2 reduce-window.6
  12.3 1.7 convolution_convert_fusion
  14.1 43.3 %all_to_all.15 = bf16[4,1,96,2048]{3,2,1,0:T(8,128)(2,1)} all-to-all(bf16[4,1,96,2048]{3,2,1,0:T(8,128)(2,1)S(1)} %bitcast.178), channel_id=1, replica_groups=mesh['grp'=2,'ep'=4,'tp'=4] {'ep'}, dimensions={0} | all-to-all | bytes 3145728 | tf_op jit(solution)/shard_map/all_to_all | solution.py:153
  59.5 3.5 %all-to-all-start.1 = ((bf16[4,192,256]{2,1,0:T(8,128)(2,1)}), bf16[4,192,256]{2,1,0:T(8,128)(2,1)S(1)}, u32[]{:S(2)}, u32[]{:S(2)}) async-start(bf16[4,192,256]{2,1,0:T(8,128)(2,1)} %stack.37), calls=%async_computation.1 | async-start | bytes 786432 | tf_op jit(solution)/shard_map/all_to_all | solution.py:60
  63.1 1.1 copy.84
  64.7 9.2 %all-to-all-done.1 = bf16[4,192,256]{2,1,0:T(8,128)(2,1)S(1)} async-done(((bf16[4,192,256]{2,1,0:T(8,128)(2,1)}), bf16[4,192,256]{2,1,0:T(8,128)(2,1)S(1)}, u32[]{:S(2)}, u32[]{:S(2)}) %all-to-all-start.1) | async-done | bytes 393248 | tf_op jit(solution)/shard_map/all_to_all | solution.py:60
  74.6 8.8 %while.18 = (s32[]{:T(128)}, f32[1,4,192]{2,1,0:T(4,128)S(1)}, f32[1,4,192]{2,1,0:T(4,128)S(1)}, f32[192,1,4,128]{3,0,2,1:T(8,128)S(1)}, bf16[768,128]{1,0:T(8,1...) while((s32[]{:T(128)}, f32[1,4,192]{2,1,0:T(4,128)S(1)}, ...), condition=%wide.region_10.11_spmd.clone, body=%wide.region_7.10_spmd.clone.sunk | while | flops 102142472 | bytes 3522743 | solution.py:103
  74.6 1.2 fusion.80
  76.3 1.2 fusion.83
  77.5 1.2 fusion.80
  79.2 1.2 fusion.83
  80.5 1.3 fusion.80
  82.2 1.2 fusion.83
  83.7 3.1 %convolution_convert_fusion.1 = bf16[192,2048]{1,0:T(8,128)(2,1)} fusion(bf16[512,2048]{1,0:T(8,128)(2,1)} %param.20, bf16[24,8,4,128]{3,2,1,0:T(4,128)(2,1)S(1)} %bitcast.185), kind=kOutput, calls=%fused_computation.35 | convolution fusion | flops 403046400 | bytes 3080192 | tf_op jit(solution)/shard_map/dot_general | solution.py:109
  86.8 16.3 %all-gather.2.cloned.1.call-done = bf16[16,1,96,2048]{3,2,1,0:T(8,128)(2,1)} async-done(((bf16[4,1,96,2048]{3,2,1,0:T(8,128)(2,1)}), bf16[16,1,96,2048]{3,2,1,0:T(8,128)(2,1)}) %all-gather.2.cloned.1.call-update) | async-done | bytes 6291472 | tf_op jit(solution)/shard_map/all_gather | solution.py:157
  103.2 8.5 %fusion.15 = f32[16,96,512]{2,1,0:T(8,128)} fusion(bf16[16,1,96,2048]{3,2,1,0:T(8,128)(2,1)} %all-gather.2.cloned.1.call-done, bf16[1,2048,512]{2,1,0:T(8,128)(2,1)} %param.26), kind=kOutput, calls=%fused_computation.22 | convolution fusion | flops 3221225472 | bytes 11534336 | tf_op jit(solution)/shard_map/secd,edf->secf/dot_general | solution.py:164
  111.7 11.9 %convert_bitcast_fusion = bf16[16,1,96,2048]{3,2,0,1:T(8,128)(2,1)} fusion(bf16[1,512,2048]{2,1,0:T(8,128)(2,1)S(1)} %copy-done, f32[16,96,512]{2,1,0:T(8,128)} %fusion.15, bf16[1,2048,512]{2,1,0:T(8,128)(2,1)} %param.25, bf16[16,1,96,2048]{3,2,1,0:T(8,128)(2,1)} %all-gather.2.cloned.1.call-done), kind=kOutput, calls=%fused_computation.26 | convolution fusion | flops 6450315264 | bytes 19922944 | tf_op jit(solution)/shard_map/secf,efd->secd/dot_general | solution.py:167
  123.6 59.0 %reduce-scatter.5.cloned.1.call-done = bf16[4,1,96,2048]{3,2,0,1:T(8,128)(2,1)} async-done(((bf16[16,1,96,2048]{3,2,0,1:T(8,128)(2,1)}), bf16[4,1,96,2048]{3,2,0,1:T(8,128)(2,1)}) %reduce-scatter.5.cloned.1.call-update) | async-done | bytes 1572880 | tf_op jit(solution)/shard_map/reduce_scatter | solution.py:166
  182.6 4.6 %all-to-all-start.2 = ((bf16[4,1,96,2048]{3,2,1,0:T(8,128)(2,1)}), bf16[4,1,96,2048]{3,2,1,0:T(8,128)(2,1)}, u32[]{:S(2)}, u32[]{:S(2)}) async-start(bf16[4,1,96,2048]{3,2,1,0:T(8,128)(2,1)} %bitcast.182), calls=%async_computation.4 | async-start | bytes 3145728 | tf_op jit(solution)/shard_map/all_to_all | solution.py:174
  188.0 36.1 %all-to-all-done.2 = bf16[4,1,96,2048]{3,2,1,0:T(8,128)(2,1)} async-done(((bf16[4,1,96,2048]{3,2,1,0:T(8,128)(2,1)}), bf16[4,1,96,2048]{3,2,1,0:T(8,128)(2,1)}, u32[]{:S(2)}, u32[]{:S(2)}) %all-to-all-start.2) | async-done | bytes 1572896 | tf_op jit(solution)/shard_map/all_to_all | solution.py:174
  224.1 1.9 convolution_multiply_fusion.2
  226.0 2.7 %fusion.24 = bf16[128,2048]{1,0:T(8,128)(2,1)} fusion(f32[128,2048]{1,0:T(8,128)S(1)} %convolution_multiply_fusion.2, bf16[384,2048]{1,0:T(8,128)(2,1)} %bitcast.36, f32[128]{0:T(128)S(1)} %get-tuple-element.216, s32[128]{0:T(128)S(1)} %get-tuple-element.232), kind=kOutput, calls=%fused_computation.39 | convolution fusion | flops 202162176 | bytes 3146752 | tf_op jit(solution)/shard_map/dot_general | solution.py:179
  (75 shorter events, 7.3 us)
Async XLA Ops:
  7.2 104.5 %copy-start = (bf16[1,512,2048]{2,1,0:T(8,128)(2,1)S(1)}, bf16[1,512,2048]{2,1,0:T(8,128)(2,1)}, u32[]{:S(2)}) copy-start(bf16[1,512,2048]{2,1,0:T(8,128)(2,1)} %param.27) | copy-start | bytes 6291460
  7.2 96.0 %all-gather.2.cloned.1.call-start = ((), (), s32[]{:S(2)}) async-start(), calls=%async_computation.5 | async-start | bytes 7864320 | tf_op jit(solution)/shard_map/all_gather | solution.py:157
  14.1 43.5 %copy-start.5 = (f32[128]{0:T(128)S(1)}, f32[128]{0:T(128)}, u32[]{:S(2)}) copy-start(f32[128]{0:T(128)} %param.18) | copy-start | bytes 1540
  14.1 43.9 %copy-start.1 = (bf16[192,128]{1,0:T(8,128)(2,1)S(1)}, bf16[192,128]{1,0:T(8,128)(2,1)}, u32[]{:S(2)}) copy-start(bf16[192,128]{1,0:T(8,128)(2,1)} %param.17) | copy-start | bytes 147460
  14.1 44.0 %copy-start.2 = (bf16[192,128]{1,0:T(8,128)(2,1)S(1)}, bf16[192,128]{1,0:T(8,128)(2,1)}, u32[]{:S(2)}) copy-start(bf16[192,128]{1,0:T(8,128)(2,1)} %param.16) | copy-start | bytes 147460
  14.1 44.2 %copy-start.4 = (f32[128]{0:T(128)S(1)}, f32[128]{0:T(128)}, u32[]{:S(2)}) copy-start(f32[128]{0:T(128)} %param.19) | copy-start | bytes 1540
  59.5 14.3 %all-to-all-start.1 = ((bf16[4,192,256]{2,1,0:T(8,128)(2,1)}), bf16[4,192,256]{2,1,0:T(8,128)(2,1)S(1)}, u32[]{:S(2)}, u32[]{:S(2)}) async-start(bf16[4,192,256]{2,1,0:T(8,128)(2,1)} %stack.37), calls=%async_computation.1 | async-start | bytes 786432 | tf_op jit(solution)/shard_map/all_to_all | solution.py:60
  63.0 119.6 %reduce-scatter.5.cloned.1.call-start = ((), (), s32[]{:S(2)}) async-start(), calls=%async_computation.7 | async-start | bytes 7864320 | tf_op jit(solution)/shard_map/reduce_scatter | solution.py:166
  123.6 64.3 %copy-start.3 = (f32[128,2]{0,1:T(2,128)S(1)}, f32[128,2]{0,1:T(2,128)}, u32[]{:S(2)}) copy-start(f32[128,2]{0,1:T(2,128)} %param.24) | copy-start | bytes 3076
  182.6 41.5 %all-to-all-start.2 = ((bf16[4,1,96,2048]{3,2,1,0:T(8,128)(2,1)}), bf16[4,1,96,2048]{3,2,1,0:T(8,128)(2,1)}, u32[]{:S(2)}, u32[]{:S(2)}) async-start(bf16[4,1,96,2048]{3,2,1,0:T(8,128)(2,1)} %bitcast.182), calls=%async_computation.4 | async-start | bytes 3145728 | tf_op jit(solution)/shard_map/all_to_all | solution.py:174
  187.2 41.5 %reduce-scatter.3.cloned.1.call-start = ((), (), s32[]{:S(2)}) async-start(), calls=%async_computation.6 | async-start | bytes 983040 | tf_op jit(solution)/shard_map/reduce_scatter | solution.py:162
Sparse Core Ops, SparseCore 0:
  57.6 45.5 all-gather.1
  123.7 58.8 reduce-scatter.4
  191.1 23.7 reduce-scatter.2
